TPU v7x, 32 devices: a whole 2x2x4 slice. The times are simulated.
32 devices in a mesh: ep: 8 (over z, y), tp: 4 (over x, core).
Axes of the slice: x: 2, y: 2, z: 4, core: 2. Of those that a mesh axis runs over, the one named last changes fastest.
Arguments:
- queries: bfloat16 [16384, 1024], P('ep', 'tp'), may hold values from -6 to 6
- keys_values: bfloat16 [16384, 512], P('ep', 'tp'), may hold values from -6 to 6
- sink_logits: float32 [16], replicated, may hold values from 4 to 8
- out_weight: bfloat16 [1024, 2048], replicated, may hold values from -4 to 4
- expert_tokens: bfloat16 [8192, 2048], P(('ep', 'tp')), may hold values from -6 to 6
- norm_gain: float32 [2048], replicated, may hold values from 0.1 to 1.9
- routes: int32 [8192, 2], P(('ep', 'tp')), may hold values from 0 to 7, all different within a row; in each aligned block of 256 rows (0 to 255, 256 to 511, ...) at most 96 rows name the same one
- route_weights: float32 [8192, 2], P(('ep', 'tp')), may hold values from 0.1 to 1
- gate_weight: bfloat16 [8, 2048, 1024], P('ep', None, 'tp'), may hold values from -0.125 to 0.125
- up_weight: bfloat16 [8, 2048, 1024], P('ep', None, 'tp'), may hold values from -0.125 to 0.125
- down_weight: bfloat16 [8, 1024, 2048], P('ep', 'tp'), may hold values from -0.1875 to 0.1875
Outputs:
- mixer_out: bfloat16 [16384, 2048], P(('ep', 'tp'))
- expert_out: bfloat16 [8192, 2048], P(('ep', 'tp'))
Inputs may be any that keep to these rules, and one draw needn't show every extreme that they name: `routes`: each row names 2 different experts. In each aligned block of 256 rows, no expert is named by more than 96 rows, and in some block an expert is named by exactly 96 rows.
All inputs are finite; a program needn't handle non-finite values.
Results may differ from a plain program's by a relative error of at most 0.012.
Values may be sent and summed in bfloat16 or wider, within the bound.
A program may use at most 128 MiB of HBM per device.

v0:
```python
import functools

import jax
import jax.numpy as jnp
from jax import lax
from jax.experimental import pallas as pl
from jax.experimental.pallas import tpu as pltpu
from jax.sharding import PartitionSpec as P

HEAD_DIM = 64
WINDOW = 128
TOPK = 2
PLANES = 4
CHUNKS = 4
STEP_ROWS = 128
NEG_FILL = -1e30
MESH = pl.DeviceIdType.MESH


def div(a, b):
    return lax.div(a, jnp.int32(b))


def rem(a, b):
    return lax.rem(a, jnp.int32(b))


def layer_kernel(n, tp, cap, stride, *refs):
    (
        sink, q_hbm, kv_hbm, ow_hbm, tok_hbm, gain, routes, rweights, gate_hbm, up_hbm, down_hbm,
        mix_hbm, out_hbm,
        tok_v, norm_v, info, info_in, block_in, x_in, near_out, relay_out, sel,
        gate_s, up_s, down_s, hid, res, relay_in, merged, near_in, far_in,
        mix_hi, mix_lo, out_v,
        q_v, kv_s, vk_s, att, att_in, ow_v, mo_v,
        load_sem, w_recv, w_near_send, w_far_send, w_fwd_send,
        halo_recv, halo_send, info_recv, info_send, block_recv, block_send,
        near_recv, near_send, pack_recv, pack_send,
        back_near_recv, back_near_send, back_far_send, back_own_send,
        relay_recv, merged_send, far_recv, att_recv, att_send, store_sem,
    ) = refs
    count, width = tok_v.shape
    wide = width // CHUNKS
    half_count = n // 2
    members = n // PLANES
    rows = half_count * stride
    group = members * stride
    side = tp // 2
    shard = gate_s.shape[2]
    seq_rows, q_width = q_v.shape
    heads = q_width // HEAD_DIM
    kv_heads = kv_s.shape[1] // (2 * HEAD_DIM)
    fan = heads // kv_heads
    own_count = seq_rows // tp

    e = lax.axis_index("ep")
    t = lax.axis_index("tp")
    plane = div(e, members)
    member = rem(e, members)
    half = div(e, half_count)
    local = rem(e, half_count)
    other = 1 - half
    is_relay = jnp.logical_or(plane == 1, plane == 2)
    own_relay_plane = 1 + half
    far_relay = (1 + other) * members + member
    tp_base = t - rem(t, side)
    tp_far = rem(t + side, tp)

    def near_tp(k):
        return tp_base + rem(t - tp_base + k, side)

    def near_ep(j):
        return rem(local + j, half_count)

    def far_source(s, k):
        return (other * 2 + s) * members + rem(member + k, members)

    def at(start, size):
        return pl.ds(pl.multiple_of(start, 16), size)

    def cols(c):
        return pl.ds(c * wide, wide)

    def remote(src, dst, send, recv, **where):
        return pltpu.make_async_remote_copy(
            src_ref=src, dst_ref=dst, send_sem=send, recv_sem=recv,
            device_id=where, device_id_type=MESH,
        )

    def arrived(ref, sem):
        pltpu.make_async_copy(ref, ref, sem).wait()

    kv_own = kv_s.at[pl.ds(WINDOW, seq_rows), :]
    loads = [
        pltpu.make_async_copy(tok_hbm, tok_v, load_sem.at[0]),
        pltpu.make_async_copy(kv_hbm, kv_own, load_sem.at[1]),
        pltpu.make_async_copy(q_hbm, q_v, load_sem.at[2]),
        pltpu.make_async_copy(ow_hbm, ow_v, load_sem.at[3]),
    ]
    items = 2 + CHUNKS

    def w_source(item):
        if item == 0:
            return gate_hbm
        if item == 1:
            return up_hbm
        return down_hbm.at[:, cols(item - 2)]

    def w_place(item, slot):
        if item == 0:
            return gate_s.at[slot]
        if item == 1:
            return up_s.at[slot]
        return down_s.at[item - 2, pl.ds(slot * shard, shard), :]

    own_weights = [
        pltpu.make_async_copy(w_source(i), w_place(i, 0), w_recv.at[i, 0]) for i in range(items)
    ]
    for copy in loads:
        copy.start()

    barrier = pltpu.get_barrier_semaphore()

    def greet(**where):
        pl.semaphore_signal(barrier, inc=1, device_id=where, device_id_type=MESH)

    for j in range(1, half_count):
        greet(ep=half * half_count + near_ep(j))
    for k in range(1, tp):
        greet(tp=rem(t + k, tp))

    @pl.when(e > 0)
    def greet_before():
        greet(ep=e - 1)

    @pl.when(e < n - 1)
    def greet_after():
        greet(ep=e + 1)

    @pl.when(is_relay)
    def greet_sources():
        for s in range(2):
            greet(ep=far_source(s, 0))

    @pl.when(jnp.logical_not(is_relay))
    def greet_relay():
        greet(ep=far_relay)

    def one(flag):
        return jnp.where(flag, 1, 0).astype(jnp.int32)

    pl.semaphore_wait(
        barrier, half_count - 1 + tp - 1 + one(e > 0) + one(e < n - 1) + 1 + one(is_relay)
    )

    halo_after = remote(
        kv_hbm.at[pl.ds(seq_rows - WINDOW, WINDOW), :], kv_s.at[pl.ds(0, WINDOW), :],
        halo_send.at[0], halo_recv.at[0], ep=rem(e + 1, n),
    )
    halo_before = remote(
        kv_hbm.at[pl.ds(0, WINDOW), :], kv_s.at[pl.ds(seq_rows + WINDOW, WINDOW), :],
        halo_send.at[1], halo_recv.at[1], ep=rem(e + n - 1, n),
    )

    @pl.when(e < n - 1)
    def send_after():
        halo_after.start()

    @pl.when(e > 0)
    def send_before():
        halo_before.start()

    w_far = [
        remote(w_source(i), w_place(i, side), w_far_send.at[i], w_recv.at[i, side], tp=tp_far)
        for i in range(items)
    ]
    w_near = [
        remote(
            w_source(i), w_place(i, (side - k) % side), w_near_send.at[i, k],
            w_recv.at[i, (side - k) % side], tp=near_tp(k),
        )
        for i in range(items)
        for k in range(1, side)
    ]
    w_fwd = {
        i: [
            remote(
                w_place(i, side), w_place(i, side + (side - k) % side), w_fwd_send.at[i, k],
                w_recv.at[i, side + (side - k) % side], tp=near_tp(k),
            )
            for k in range(1, side)
        ]
        for i in range(items)
    }
    for copy in w_far:
        copy.start()

    loads[0].wait()
    tokens = tok_v[...].astype(jnp.float32)
    centred = tokens - jnp.mean(tokens, -1, keepdims=True)
    scale = lax.rsqrt(jnp.mean(centred * centred, -1, keepdims=True) + 1e-06)
    normed = (centred * scale * gain[...]).astype(jnp.bfloat16)
    for c in range(CHUNKS):
        norm_v[c] = normed[:, c * wide : (c + 1) * wide]

    expert = lax.broadcasted_iota(jnp.int32, (n, count), 0)
    named = [expert == routes[k : k + 1, :] for k in range(TOPK)]
    member_of = functools.reduce(jnp.logical_or, named)
    earlier = lax.broadcasted_iota(jnp.int32, (count, count), 0) < lax.broadcasted_iota(
        jnp.int32, (count, count), 1
    )
    rank = jnp.dot(
        jnp.where(member_of, 1.0, 0.0).astype(jnp.bfloat16),
        jnp.where(earlier, 1.0, 0.0).astype(jnp.bfloat16),
        preferred_element_type=jnp.float32,
    )
    place = expert.astype(jnp.float32) * float(stride) + rank
    info[...] = jnp.zeros_like(info)
    for k in range(TOPK):
        info[k : k + 1, :] = jnp.sum(jnp.where(named[k], place, 0.0), 0, keepdims=True)
        info[TOPK + k : TOPK + k + 1, :] = rweights[k : k + 1, :]

    slot_of = rem(plane, 2)
    send_info = remote(info, info_in.at[slot_of], info_send, info_recv.at[slot_of], ep=far_relay)
    send_info.start()
    send_blocks = [
        remote(
            norm_v.at[c], block_in.at[slot_of, c], block_send.at[c], block_recv.at[slot_of, c],
            ep=far_relay,
        )
        for c in range(CHUNKS)
    ]
    for copy in send_blocks:
        copy.start()
    for copy in w_near:
        copy.start()
    for copy in own_weights:
        copy.start()

    base = half * rows

    def hits(table, k):
        slot = lax.broadcasted_iota(jnp.int32, (rows, count), 0) + base
        return slot.astype(jnp.float32) == table[k : k + 1, :]

    def pick(table):
        hit = functools.reduce(jnp.logical_or, [hits(table, k) for k in range(TOPK)])
        return jnp.where(hit, 1.0, 0.0).astype(jnp.bfloat16)

    def mixture(table, where):
        mix = sum(
            jnp.where(hits(table, k), table[TOPK + k : TOPK + k + 1, :], 0.0)
            for k in range(TOPK)
        ).T
        high = mix.astype(jnp.bfloat16)
        mix_hi[where] = high
        mix_lo[where] = (mix - high.astype(jnp.float32)).astype(jnp.bfloat16)

    own_table = info[...]
    sel[2] = pick(own_table)
    for c in range(CHUNKS):
        near_out[:, cols(c)] = jnp.dot(
            sel[2], norm_v[c], preferred_element_type=jnp.float32
        ).astype(jnp.bfloat16)
    own_rows = at(e * stride, stride)
    near_self = pltpu.make_async_copy(
        near_out.at[at(local * stride, stride), :], x_in.at[own_rows, :], near_recv
    )
    near_self.start()
    for j in range(1, half_count):
        remote(
            near_out.at[at(near_ep(j) * stride, stride), :], x_in.at[own_rows, :],
            near_send, near_recv, ep=half * half_count + near_ep(j),
        ).start()
    mixture(own_table, 2)

    loads[1].wait()

    @pl.when(e == 0)
    def no_before():
        kv_s[0:WINDOW, :] = jnp.zeros((WINDOW, kv_s.shape[1]), kv_s.dtype)

    @pl.when(e > 0)
    def got_before():
        halo_after.wait_recv()

    @pl.when(e == n - 1)
    def no_after():
        kv_s[seq_rows + WINDOW : seq_rows + 2 * WINDOW, :] = jnp.zeros(
            (WINDOW, kv_s.shape[1]), kv_s.dtype
        )

    @pl.when(e < n - 1)
    def got_after():
        halo_before.wait_recv()

    for kv_head in range(kv_heads):
        lanes = slice(kv_head * 2 * HEAD_DIM, (kv_head + 1) * 2 * HEAD_DIM)
        both = kv_s[:, lanes]
        vk_s[:, lanes] = jnp.concatenate([both[:, HEAD_DIM:], both[:, :HEAD_DIM]], 1)
    loads[2].wait()

    span = STEP_ROWS + 2 * WINDOW
    seq_total = seq_rows * n
    lower = lax.broadcasted_iota(jnp.int32, (STEP_ROWS, 2 * HEAD_DIM), 1) < HEAD_DIM

    def attend_step(start):
        start = pl.multiple_of(start, STEP_ROWS)
        row = lax.broadcasted_iota(jnp.int32, (STEP_ROWS, span), 0)
        column = lax.broadcasted_iota(jnp.int32, (STEP_ROWS, span), 1)
        key_pos = e * seq_rows + start - WINDOW + column
        allowed = (
            (column >= row) & (column <= row + 2 * WINDOW)
            & (key_pos >= 0) & (key_pos < seq_total)
        )
        for kv_head in range(kv_heads):
            lanes = slice(kv_head * 2 * HEAD_DIM, (kv_head + 1) * 2 * HEAD_DIM)
            kv = kv_s[pl.ds(start, span), lanes]
            vk = vk_s[pl.ds(start, span), lanes]
            for pair in range(fan // 2):
                head = kv_head * fan + 2 * pair
                places = slice(head * HEAD_DIM, (head + 2) * HEAD_DIM)
                q_pair = q_v[pl.ds(start, STEP_ROWS), places] * jnp.bfloat16(HEAD_DIM ** -0.5)
                results = []
                for odd in range(2):
                    q_one = jnp.where(lower != bool(odd), q_pair, jnp.zeros_like(q_pair))
                    key_side, value_side = (vk, kv) if odd else (kv, vk)
                    scores = lax.dot_general(
                        q_one, key_side, (((1,), (1,)), ((), ())),
                        preferred_element_type=jnp.float32,
                    )
                    scores = jnp.where(allowed, scores, NEG_FILL)
                    bound = sink[t * heads + head + odd]
                    top = jnp.maximum(jnp.max(scores, 1, keepdims=True), bound)
                    expo = jnp.exp(scores - top)
                    denom = jnp.sum(expo, 1, keepdims=True) + jnp.exp(bound - top)
                    value = jnp.dot(
                        expo.astype(jnp.bfloat16), value_side, preferred_element_type=jnp.float32
                    )
                    results.append(value / denom)
                att[pl.ds(start, STEP_ROWS), places] = jnp.where(
                    lower, results[0], results[1]
                ).astype(jnp.bfloat16)

    def attend_block(k):
        owner = rem(t + k, tp)

        def step(i, carry):
            attend_step(owner * own_count + i * STEP_ROWS)
            return carry

        lax.fori_loop(0, own_count // STEP_ROWS, step, 0)
        block = att.at[at(owner * own_count, own_count), :]
        if k == 0:
            pltpu.make_async_copy(block, att_in.at[t], att_recv.at[0]).start()
        else:
            remote(block, att_in.at[t], att_send.at[k], att_recv.at[k], tp=owner).start()

    def relay_tables():
        for s in range(2):
            arrived(info_in.at[s], info_recv.at[s])
            table = info_in[s]
            sel[s] = pick(table)
            mixture(table, s)

    def relay_forward(c):
        for s in (1, 0):
            arrived(block_in.at[s, c], block_recv.at[s, c])
            relay_out[s, c] = jnp.dot(
                sel[s], block_in[s, c], preferred_element_type=jnp.float32
            ).astype(jnp.bfloat16)
            landing = x_in.at[at(far_source(s, 0) * stride, stride), cols(c)]
            for j in list(range(1, half_count)):
                remote(
                    relay_out.at[s, c, at(near_ep(j) * stride, stride), :], landing,
                    pack_send.at[s, c], pack_recv.at[s], ep=half * half_count + near_ep(j),
                ).start()
            pltpu.make_async_copy(
                relay_out.at[s, c, at(local * stride, stride), :], landing, pack_recv.at[s]
            ).start()

    def on_relay(task, *args):
        pl.when(is_relay)(lambda: task(*args))

    def forward_weights(i):
        arrived(w_place(i, side), w_recv.at[i, side])
        for copy in w_fwd[i]:
            copy.start()

    def hidden_rows(start, size, slot):
        x = x_in[at(start, size), :]
        gate = jnp.dot(x, gate_s[slot], preferred_element_type=jnp.float32)
        up = jnp.dot(x, up_s[slot], preferred_element_type=jnp.float32)
        hid[at(start, size), pl.ds(slot * shard, shard)] = (
            gate / (1.0 + jnp.exp(-gate)) * up
        ).astype(jnp.bfloat16)

    def got_weights(item, slot):
        arrived(w_place(item, slot), w_recv.at[item, slot])

    def project():
        arrived(att_in.at[0], att_recv.at[0])
        for k in range(1, tp):
            arrived(att_in.at[0], att_recv.at[k])
        loads[3].wait()
        total = jnp.zeros(mo_v.shape, jnp.float32)
        for c in range(CHUNKS):
            total = sum(
                jnp.dot(
                    att_in[k], ow_v[k * q_width : (k + 1) * q_width, cols(c)],
                    preferred_element_type=jnp.float32,
                )
                for k in range(tp)
            )
            mo_v[:, cols(c)] = total.astype(jnp.bfloat16)
        pltpu.make_async_copy(mo_v, mix_hbm, store_sem.at[CHUNKS]).start()

    on_relay(relay_tables)
    for k in range(1, 3):
        attend_block(k)
    on_relay(relay_forward, 0)
    for k in range(3, tp):
        attend_block(k)
    forward_weights(0)
    on_relay(relay_forward, 1)
    attend_block(0)
    for slot in range(side):
        for item in range(2):
            got_weights(item, slot)
    on_relay(relay_forward, 2)
    project()
    arrived(x_in.at[at(half * rows, rows), :], near_recv)
    for slot in range(side):
        hidden_rows(half * rows, rows, slot)
    forward_weights(1)
    on_relay(relay_forward, 3)
    for c in range(4, CHUNKS):
        on_relay(relay_forward, c)
    for slot in range(side, tp):
        for item in range(2):
            if slot > side:
                got_weights(item, slot)
        hidden_rows(half * rows, rows, slot)
    forward_weights(2)
    for s in (1, 0):
        arrived(x_in.at[at((other * 2 + s) * group, group), :], pack_recv.at[s])
    for slot in range(tp):
        hidden_rows(other * rows, rows, slot)

    def results(c):
        for slot in range(tp):
            if slot != side:
                got_weights(2 + c, slot)
        res[c] = jnp.dot(hid[...], down_s[c], preferred_element_type=jnp.float32).astype(
            jnp.bfloat16
        )
        for s in range(2):
            for k in range(members):
                block = res.at[c, at(far_source(s, k) * stride, stride), :]
                landing = relay_in.at[s, c, at(local * stride, stride), :]
                relay = own_relay_plane * members + rem(member + k, members)
                if k:
                    remote(
                        block, landing, back_far_send.at[c], relay_recv.at[s, c], ep=relay
                    ).start()
                else:

                    @pl.when(is_relay)
                    def keep():
                        pltpu.make_async_copy(block, landing, relay_recv.at[s, c]).start()

                    @pl.when(jnp.logical_not(is_relay))
                    def send():
                        remote(
                            block, landing, back_own_send.at[c], relay_recv.at[s, c], ep=relay
                        ).start()

        landing = near_in.at[c, at(local * stride, stride), :]
        for j in range(1, half_count):
            target = half * half_count + near_ep(j)
            remote(
                res.at[c, at(target * stride, stride), :], landing,
                back_near_send.at[c], back_near_recv.at[c], ep=target,
            ).start()
        pltpu.make_async_copy(
            res.at[c, own_rows, :], landing, back_near_recv.at[c]
        ).start()

    def mixed(where, values):
        return jnp.dot(
            mix_hi[where], values, preferred_element_type=jnp.float32
        ) + jnp.dot(mix_lo[where], values, preferred_element_type=jnp.float32)

    def relay_merge(c):
        for s in range(2):
            arrived(relay_in.at[s, c], relay_recv.at[s, c])
            merged[s, c] = mixed(s, relay_in[s, c]).astype(jnp.bfloat16)
            remote(
                merged.at[s, c], far_in.at[c], merged_send.at[s, c], far_recv.at[c],
                ep=far_source(s, 0),
            ).start()

    def finish(c):
        arrived(near_in.at[c], back_near_recv.at[c])
        total = mixed(2, near_in[c])
        arrived(far_in.at[c], far_recv.at[c])
        out_v[:, cols(c)] = (total + far_in[c].astype(jnp.float32)).astype(jnp.bfloat16)
        pltpu.make_async_copy(
            out_v.at[:, cols(c)], out_hbm.at[:, cols(c)], store_sem.at[c]
        ).start()

    for step in range(CHUNKS + 4):
        if step < CHUNKS:
            results(step)
        if step + 1 < CHUNKS:
            forward_weights(2 + step + 1)
        if 1 <= step <= CHUNKS:
            on_relay(relay_merge, step - 1)
        if 3 <= step < CHUNKS + 3:
            finish(step - 3)

    for c in range(CHUNKS):
        pltpu.make_async_copy(
            out_v.at[:, cols(c)], out_hbm.at[:, cols(c)], store_sem.at[c]
        ).wait()
    pltpu.make_async_copy(mo_v, mix_hbm, store_sem.at[CHUNKS]).wait()

    def sent(ref, sem):
        pltpu.make_async_copy(ref, ref, sem).wait()

    @pl.when(e < n - 1)
    def sent_after():
        halo_after.wait_send()

    @pl.when(e > 0)
    def sent_before():
        halo_before.wait_send()

    for copy in w_far + w_near + [c for i in range(items) for c in w_fwd[i]]:
        copy.wait_send()
    send_info.wait_send()
    for copy in send_blocks:
        copy.wait_send()
    others = half_count - 1
    sent(near_out.at[pl.ds(0, others * stride), :], near_send)
    for k in range(1, tp):
        sent(att_in.at[0], att_send.at[k])
    for c in range(CHUNKS):
        sent(near_in.at[c, pl.ds(0, others * stride), :], back_near_send.at[c])
        sent(res.at[c, pl.ds(0, 2 * (members - 1) * stride), :], back_far_send.at[c])

        @pl.when(is_relay)
        def sent_relay():
            for s in range(2):
                sent(relay_out.at[s, c, pl.ds(0, others * stride), :], pack_send.at[s, c])
                sent(merged.at[s, c], merged_send.at[s, c])

        @pl.when(jnp.logical_not(is_relay))
        def sent_own():
            sent(res.at[c, pl.ds(0, 2 * stride), :], back_own_send.at[c])


def body(
    queries,
    keys_values,
    sink_logits,
    out_weight,
    expert_tokens,
    norm_gain,
    routes,
    route_weights,
    gate_weight,
    up_weight,
    down_weight,
):
    n, tp = lax.axis_size("ep"), lax.axis_size("tp")
    count, width = expert_tokens.shape
    cap = 3 * count * TOPK // (2 * n)
    stride = -(-cap // 16) * 16
    rows = n // 2 * stride
    wide = width // CHUNKS
    shard = gate_weight.shape[2]
    seq_rows, q_width = queries.shape
    kv_width = keys_values.shape[1]
    items = 2 + CHUNKS
    side = tp // 2
    bf16, f32 = jnp.bfloat16, jnp.float32
    dma = pltpu.SemaphoreType.DMA

    def vmem(*shape, dtype=bf16):
        return pltpu.VMEM(shape, dtype)

    scratch = [
        vmem(count, width),
        vmem(CHUNKS, count, wide),
        vmem(8, count, dtype=f32),
        vmem(2, 8, count, dtype=f32),
        vmem(2, CHUNKS, count, wide),
        vmem(n * stride, width),
        vmem(rows, width),
        vmem(2, CHUNKS, rows, wide),
        vmem(3, rows, count),
        vmem(tp, width, shard),
        vmem(tp, width, shard),
        vmem(CHUNKS, tp * shard, wide),
        vmem(n * stride, tp * shard),
        vmem(CHUNKS, n * stride, wide),
        vmem(2, CHUNKS, rows, wide),
        vmem(2, CHUNKS, count, wide),
        vmem(CHUNKS, rows, wide),
        vmem(CHUNKS, count, wide),
        vmem(3, count, rows),
        vmem(3, count, rows),
        vmem(count, width),
        vmem(seq_rows, q_width),
        vmem(seq_rows + 2 * WINDOW, kv_width),
        vmem(seq_rows + 2 * WINDOW, kv_width),
        vmem(seq_rows, q_width),
        vmem(tp, seq_rows // tp, q_width),
        vmem(*out_weight.shape),
        vmem(seq_rows // tp, width),
        dma((4,)),
        dma((items, tp)),
        dma((items, side)),
        dma((items,)),
        dma((items, side)),
        dma((2,)),
        dma((2,)),
        dma((2,)),
        dma,
        dma((2, CHUNKS)),
        dma((CHUNKS,)),
        dma,
        dma,
        dma((2,)),
        dma((2, CHUNKS)),
        dma((CHUNKS,)),
        dma((CHUNKS,)),
        dma((CHUNKS,)),
        dma((CHUNKS,)),
        dma((2, CHUNKS)),
        dma((2, CHUNKS)),
        dma((CHUNKS,)),
        dma((tp,)),
        dma((tp,)),
        dma((CHUNKS + 1,)),
    ]
    anywhere = pl.BlockSpec(memory_space=pl.ANY)
    small = pl.BlockSpec(memory_space=pltpu.VMEM)
    return pl.pallas_call(
        functools.partial(layer_kernel, n, tp, cap, stride),
        out_shape=(
            jax.ShapeDtypeStruct((seq_rows // tp, width), bf16),
            jax.ShapeDtypeStruct((count, width), bf16),
        ),
        in_specs=[
            pl.BlockSpec(memory_space=pltpu.SMEM), anywhere, anywhere, anywhere, anywhere,
            small, small, small, anywhere, anywhere, anywhere,
        ],
        out_specs=(anywhere, anywhere),
        scratch_shapes=scratch,
        compiler_params=pltpu.CompilerParams(
            collective_id=0, has_side_effects=True, vmem_limit_bytes=67043328
        ),
        name="layer",
    )(
        sink_logits, queries, keys_values, out_weight, expert_tokens,
        norm_gain.reshape(1, width), routes.T, route_weights.T,
        gate_weight[0], up_weight[0], down_weight[0],
    )


def solution(mesh):
    return jax.shard_map(
        body,
        mesh=mesh,
        in_specs=(
            P("ep", "tp"),
            P("ep", "tp"),
            P(),
            P(),
            P(("ep", "tp"), None),
            P(),
            P(("ep", "tp"), None),
            P(("ep", "tp"), None),
            P("ep", None, "tp"),
            P("ep", None, "tp"),
            P("ep", "tp", None),
        ),
        out_specs=(P(("ep", "tp"), None), P(("ep", "tp"), None)),
        check_vma=False,
    )
```

profile of v0, /device:TPU:9, one launch (start us, length us, event | category | flops | bytes accessed | tf_op | source)
XLA Modules:
  0.0 162.4 jit_solution(13459855087541876569)
XLA Ops:
  0.6 157.5 %layer.1 = (bf16[512,2048]{1,0:T(8,128)(2,1)}, bf16[256,2048]{1,0:T(8,128)(2,1)}) custom-call(f32[16]{0:T(128)} %refs_0_.1, bf16[2048,256]{1,0:T(8,128)(2,1)} %refs_1_.1, bf16[2048,128]{1,0:T(8,128)(2,1)} %refs_2_.1, bf16[1024,2048]{1,0:T(8,128)(2,1)} %refs_3_.1, bf16[256,2048]{1,0:T(8,128)(2,1)} %refs_4_.1, f32[1,2048]{1,0:T(1,128)} %bitcast.9, ...), custom_call_target="tpu_custom_call" | custom-call | tf_op jit(solution)/shard_map/layer/pallas_call | solution.py:650
  158.2 0.0 copy-start
  158.2 3.2 %copy.15 = bf16[512,2048]{1,0:T(8,128)(2,1)} copy(bf16[512,2048]{1,0:T(8,128)(2,1)} %get-tuple-element.4) | data formatting | bytes 4194304
  161.4 0.0 copy-done
  161.4 1.0 copy.16
Async XLA Ops:
  158.2 3.3 %copy-start = (bf16[256,2048]{1,0:T(8,128)(2,1)S(1)}, bf16[256,2048]{1,0:T(8,128)(2,1)}, u32[]{:S(2)}) copy-start(bf16[256,2048]{1,0:T(8,128)(2,1)} %get-tuple-element.5) | copy-start | bytes 3145732
where the time goes:
time: 163 us; the launch traced here: 162 us
  Pallas kernels  158 us (97%)
  local copies, waits for them, and re-layouts  4.22 us (3%)
    pallas_call x1, Pallas kernels, body(): pl.pallas_call(functools.partial(layer_kernel, n, tp, cap, stride), out_s...  158 us
    unnamed x4, local copies, waits for them, and re-layouts  4.22 us

commit v1 on v0

--- a/solution.py
+++ b/solution.py
@@ -11,7 +11,7 @@
 WINDOW = 128
 TOPK = 2
 PLANES = 4
-CHUNKS = 4
+CHUNKS = 8
 STEP_ROWS = 128
 NEG_FILL = -1e30
 MESH = pl.DeviceIdType.MESH
@@ -72,8 +72,11 @@
     def near_ep(j):
         return rem(local + j, half_count)
 
+    def far_plane(s):
+        return 1 + other if s else 3 * other
+
     def far_source(s, k):
-        return (other * 2 + s) * members + rem(member + k, members)
+        return far_plane(s) * members + rem(member + k, members)
 
     def at(start, size):
         return pl.ds(pl.multiple_of(start, 16), size)
@@ -220,7 +223,7 @@
         info[k : k + 1, :] = jnp.sum(jnp.where(named[k], place, 0.0), 0, keepdims=True)
         info[TOPK + k : TOPK + k + 1, :] = rweights[k : k + 1, :]
 
-    slot_of = rem(plane, 2)
+    slot_of = one(is_relay)
     send_info = remote(info, info_in.at[slot_of], info_send, info_recv.at[slot_of], ep=far_relay)
     send_info.start()
     send_blocks = [
@@ -363,21 +366,20 @@
             sel[s] = pick(table)
             mixture(table, s)
 
-    def relay_forward(c):
-        for s in (1, 0):
-            arrived(block_in.at[s, c], block_recv.at[s, c])
-            relay_out[s, c] = jnp.dot(
-                sel[s], block_in[s, c], preferred_element_type=jnp.float32
-            ).astype(jnp.bfloat16)
-            landing = x_in.at[at(far_source(s, 0) * stride, stride), cols(c)]
-            for j in list(range(1, half_count)):
-                remote(
-                    relay_out.at[s, c, at(near_ep(j) * stride, stride), :], landing,
-                    pack_send.at[s, c], pack_recv.at[s], ep=half * half_count + near_ep(j),
-                ).start()
-            pltpu.make_async_copy(
-                relay_out.at[s, c, at(local * stride, stride), :], landing, pack_recv.at[s]
+    def relay_forward(s, c):
+        arrived(block_in.at[s, c], block_recv.at[s, c])
+        relay_out[s, c] = jnp.dot(
+            sel[s], block_in[s, c], preferred_element_type=jnp.float32
+        ).astype(jnp.bfloat16)
+        landing = x_in.at[at(far_source(s, 0) * stride, stride), cols(c)]
+        for j in range(1, half_count):
+            remote(
+                relay_out.at[s, c, at(near_ep(j) * stride, stride), :], landing,
+                pack_send.at[s, c], pack_recv.at[s], ep=half * half_count + near_ep(j),
             ).start()
+        pltpu.make_async_copy(
+            relay_out.at[s, c, at(local * stride, stride), :], landing, pack_recv.at[s]
+        ).start()
 
     def on_relay(task, *args):
         pl.when(is_relay)(lambda: task(*args))
@@ -415,66 +417,36 @@
             mo_v[:, cols(c)] = total.astype(jnp.bfloat16)
         pltpu.make_async_copy(mo_v, mix_hbm, store_sem.at[CHUNKS]).start()
 
-    on_relay(relay_tables)
-    for k in range(1, 3):
-        attend_block(k)
-    on_relay(relay_forward, 0)
-    for k in range(3, tp):
-        attend_block(k)
-    forward_weights(0)
-    on_relay(relay_forward, 1)
-    attend_block(0)
-    for slot in range(side):
-        for item in range(2):
-            got_weights(item, slot)
-    on_relay(relay_forward, 2)
-    project()
-    arrived(x_in.at[at(half * rows, rows), :], near_recv)
-    for slot in range(side):
-        hidden_rows(half * rows, rows, slot)
-    forward_weights(1)
-    on_relay(relay_forward, 3)
-    for c in range(4, CHUNKS):
-        on_relay(relay_forward, c)
-    for slot in range(side, tp):
-        for item in range(2):
-            if slot > side:
-                got_weights(item, slot)
-        hidden_rows(half * rows, rows, slot)
-    forward_weights(2)
-    for s in (1, 0):
-        arrived(x_in.at[at((other * 2 + s) * group, group), :], pack_recv.at[s])
-    for slot in range(tp):
-        hidden_rows(other * rows, rows, slot)
-
-    def results(c):
-        for slot in range(tp):
-            if slot != side:
-                got_weights(2 + c, slot)
-        res[c] = jnp.dot(hid[...], down_s[c], preferred_element_type=jnp.float32).astype(
-            jnp.bfloat16
-        )
-        for s in range(2):
-            for k in range(members):
-                block = res.at[c, at(far_source(s, k) * stride, stride), :]
-                landing = relay_in.at[s, c, at(local * stride, stride), :]
-                relay = own_relay_plane * members + rem(member + k, members)
-                if k:
+    def results(s, c):
+        first = far_plane(s) * group
+        res[c, at(first, group), :] = jnp.dot(
+            hid[at(first, group), :], down_s[c], preferred_element_type=jnp.float32
+        ).astype(jnp.bfloat16)
+        for k in range(members):
+            block = res.at[c, at(far_source(s, k) * stride, stride), :]
+            landing = relay_in.at[s, c, at(local * stride, stride), :]
+            relay = own_relay_plane * members + rem(member + k, members)
+            if k:
+                remote(
+                    block, landing, back_far_send.at[s, c], relay_recv.at[s, c], ep=relay
+                ).start()
+            else:
+
+                @pl.when(is_relay)
+                def keep():
+                    pltpu.make_async_copy(block, landing, relay_recv.at[s, c]).start()
+
+                @pl.when(jnp.logical_not(is_relay))
+                def send():
                     remote(
-                        block, landing, back_far_send.at[c], relay_recv.at[s, c], ep=relay
+                        block, landing, back_own_send.at[s, c], relay_recv.at[s, c], ep=relay
                     ).start()
-                else:
-
-                    @pl.when(is_relay)
-                    def keep():
-                        pltpu.make_async_copy(block, landing, relay_recv.at[s, c]).start()
-
-                    @pl.when(jnp.logical_not(is_relay))
-                    def send():
-                        remote(
-                            block, landing, back_own_send.at[c], relay_recv.at[s, c], ep=relay
-                        ).start()
-
+
+    def near_results(c):
+        first = half * rows
+        res[c, at(first, rows), :] = jnp.dot(
+            hid[at(first, rows), :], down_s[c], preferred_element_type=jnp.float32
+        ).astype(jnp.bfloat16)
         landing = near_in.at[c, at(local * stride, stride), :]
         for j in range(1, half_count):
             target = half * half_count + near_ep(j)
@@ -491,14 +463,13 @@
             mix_hi[where], values, preferred_element_type=jnp.float32
         ) + jnp.dot(mix_lo[where], values, preferred_element_type=jnp.float32)
 
-    def relay_merge(c):
-        for s in range(2):
-            arrived(relay_in.at[s, c], relay_recv.at[s, c])
-            merged[s, c] = mixed(s, relay_in[s, c]).astype(jnp.bfloat16)
-            remote(
-                merged.at[s, c], far_in.at[c], merged_send.at[s, c], far_recv.at[c],
-                ep=far_source(s, 0),
-            ).start()
+    def relay_merge(s, c):
+        arrived(relay_in.at[s, c], relay_recv.at[s, c])
+        merged[s, c] = mixed(s, relay_in[s, c]).astype(jnp.bfloat16)
+        remote(
+            merged.at[s, c], far_in.at[c], merged_send.at[s, c], far_recv.at[c],
+            ep=far_source(s, 0),
+        ).start()
 
     def finish(c):
         arrived(near_in.at[c], back_near_recv.at[c])
@@ -509,15 +480,83 @@
             out_v.at[:, cols(c)], out_hbm.at[:, cols(c)], store_sem.at[c]
         ).start()
 
-    for step in range(CHUNKS + 4):
-        if step < CHUNKS:
-            results(step)
-        if step + 1 < CHUNKS:
-            forward_weights(2 + step + 1)
-        if 1 <= step <= CHUNKS:
-            on_relay(relay_merge, step - 1)
-        if 3 <= step < CHUNKS + 3:
-            finish(step - 3)
+    on_relay(relay_tables)
+    attend_block(1)
+    for c in range(0, 2):
+        on_relay(relay_forward, 0, c)
+    attend_block(2)
+    for c in range(2, 4):
+        on_relay(relay_forward, 0, c)
+    for k in range(3, tp):
+        attend_block(k)
+    on_relay(relay_forward, 0, 4)
+    attend_block(0)
+    for c in range(5, CHUNKS):
+        on_relay(relay_forward, 0, c)
+    forward_weights(0)
+    for slot in range(side):
+        for item in range(2):
+            got_weights(item, slot)
+    for c in range(0, 4):
+        on_relay(relay_forward, 1, c)
+    first_rows, last_rows = far_plane(0) * group, far_plane(1) * group
+    arrived(x_in.at[at(first_rows, group), :], pack_recv.at[0])
+    for slot in range(side):
+        hidden_rows(first_rows, group, slot)
+    for c in range(4, 6):
+        on_relay(relay_forward, 1, c)
+    arrived(x_in.at[at(half * rows, rows), :], near_recv)
+    for slot in range(side):
+        hidden_rows(half * rows, rows, slot)
+    on_relay(relay_forward, 1, 6)
+    forward_weights(1)
+    hidden_rows(first_rows, group, side)
+    for c in range(7, CHUNKS):
+        on_relay(relay_forward, 1, c)
+    for slot in range(side + 1, tp):
+        for item in range(2):
+            got_weights(item, slot)
+        hidden_rows(first_rows, group, slot)
+
+    def got_down(c):
+        for slot in range(tp):
+            if slot != side:
+                got_weights(2 + c, slot)
+
+    forward_weights(2)
+    hidden_rows(half * rows, rows, side)
+    got_down(0)
+    results(0, 0)
+    forward_weights(3)
+    for slot in range(side + 1, tp):
+        hidden_rows(half * rows, rows, slot)
+    got_down(1)
+    results(0, 1)
+    arrived(x_in.at[at(last_rows, group), :], pack_recv.at[1])
+    for slot in range(tp):
+        hidden_rows(last_rows, group, slot)
+    results(1, 0)
+    results(1, 1)
+    merges = [(0, 0), (0, 1), (1, 0), (1, 1)] + [
+        (s, c) for c in range(2, CHUNKS) for s in range(2)
+    ]
+    due = {3: 3, 4: 1, 5: 1, 6: 2, 7: 1}
+    for c in range(2, CHUNKS):
+        forward_weights(2 + c)
+        got_down(c)
+        results(0, c)
+        results(1, c)
+        for _ in range(due.get(c, 0)):
+            on_relay(relay_merge, *merges.pop(0))
+    for c in range(0, CHUNKS, 2):
+        near_results(c)
+        near_results(c + 1)
+        on_relay(relay_merge, *merges.pop(0))
+    project()
+    for item in merges:
+        on_relay(relay_merge, *item)
+    for c in range(CHUNKS):
+        finish(c)
 
     for c in range(CHUNKS):
         pltpu.make_async_copy(
@@ -547,7 +586,8 @@
         sent(att_in.at[0], att_send.at[k])
     for c in range(CHUNKS):
         sent(near_in.at[c, pl.ds(0, others * stride), :], back_near_send.at[c])
-        sent(res.at[c, pl.ds(0, 2 * (members - 1) * stride), :], back_far_send.at[c])
+        for s in range(2):
+            sent(res.at[c, pl.ds(0, (members - 1) * stride), :], back_far_send.at[s, c])
 
         @pl.when(is_relay)
         def sent_relay():
@@ -557,7 +597,8 @@
 
         @pl.when(jnp.logical_not(is_relay))
         def sent_own():
-            sent(res.at[c, pl.ds(0, 2 * stride), :], back_own_send.at[c])
+            for s in range(2):
+                sent(res.at[c, pl.ds(0, stride), :], back_own_send.at[s, c])
 
 
 def body(
@@ -636,8 +677,8 @@
         dma((2, CHUNKS)),
         dma((CHUNKS,)),
         dma((CHUNKS,)),
-        dma((CHUNKS,)),
-        dma((CHUNKS,)),
+        dma((2, CHUNKS)),
+        dma((2, CHUNKS)),
         dma((2, CHUNKS)),
         dma((2, CHUNKS)),
         dma((CHUNKS,)),

time: 163 us -> 129 us (0.79)
  the two profiles are of different devices: /device:TPU:9 before, /device:TPU:0 now
where the time goes in v1:
time: 129 us
  Pallas kernels  124 us (96%)
  local copies, waits for them, and re-layouts  4.22 us (3%)
    pallas_call x1, Pallas kernels, body(): pl.pallas_call(functools.partial(layer_kernel, n, tp, cap, stride), out_s...  124 us
    unnamed x4, local copies, waits for them, and re-layouts  4.22 us

profile of v1, /device:TPU:0, one launch (start us, length us, event | category | flops | bytes accessed | tf_op | source)
XLA Modules:
  0.0 129.0 jit_solution(1390890817145616843)
XLA Ops:
  0.6 124.1 %layer.1 = (bf16[512,2048]{1,0:T(8,128)(2,1)}, bf16[256,2048]{1,0:T(8,128)(2,1)}) custom-call(f32[16]{0:T(128)} %refs_0_.1, bf16[2048,256]{1,0:T(8,128)(2,1)} %refs_1_.1, bf16[2048,128]{1,0:T(8,128)(2,1)} %refs_2_.1, bf16[1024,2048]{1,0:T(8,128)(2,1)} %refs_3_.1, bf16[256,2048]{1,0:T(8,128)(2,1)} %refs_4_.1, f32[1,2048]{1,0:T(1,128)} %bitcast.9, ...), custom_call_target="tpu_custom_call" | custom-call | tf_op jit(solution)/shard_map/layer/pallas_call | solution.py:691
  124.7 0.0 copy-start
  124.8 3.2 %copy.15 = bf16[512,2048]{1,0:T(8,128)(2,1)} copy(bf16[512,2048]{1,0:T(8,128)(2,1)} %get-tuple-element.4) | data formatting | bytes 4194304
  128.0 0.0 copy-done
  128.0 1.0 copy.16
Async XLA Ops:
  124.7 3.3 %copy-start = (bf16[256,2048]{1,0:T(8,128)(2,1)S(1)}, bf16[256,2048]{1,0:T(8,128)(2,1)}, u32[]{:S(2)}) copy-start(bf16[256,2048]{1,0:T(8,128)(2,1)} %get-tuple-element.5) | copy-start | bytes 3145732

commit v2 on v1

--- a/solution.py
+++ b/solution.py
@@ -36,7 +36,7 @@
         load_sem, w_recv, w_near_send, w_far_send, w_fwd_send,
         halo_recv, halo_send, info_recv, info_send, block_recv, block_send,
         near_recv, near_send, pack_recv, pack_send,
-        back_near_recv, back_near_send, back_far_send, back_own_send,
+        back_near_recv, back_near_send, back_far_send, edge_send,
         relay_recv, merged_send, far_recv, att_recv, att_send, store_sem,
     ) = refs
     count, width = tok_v.shape
@@ -277,30 +277,38 @@
         ).start()
     mixture(own_table, 2)
 
+    def both_orders(first, size):
+        for kv_head in range(kv_heads):
+            lanes = slice(kv_head * 2 * HEAD_DIM, (kv_head + 1) * 2 * HEAD_DIM)
+            both = kv_s[first : first + size, lanes]
+            vk_s[first : first + size, lanes] = jnp.concatenate(
+                [both[:, HEAD_DIM:], both[:, :HEAD_DIM]], 1
+            )
+
+    def got_halo():
+        @pl.when(e == 0)
+        def no_before():
+            kv_s[0:WINDOW, :] = jnp.zeros((WINDOW, kv_s.shape[1]), kv_s.dtype)
+
+        @pl.when(e > 0)
+        def got_before():
+            halo_after.wait_recv()
+
+        @pl.when(e == n - 1)
+        def no_after():
+            kv_s[seq_rows + WINDOW : seq_rows + 2 * WINDOW, :] = jnp.zeros(
+                (WINDOW, kv_s.shape[1]), kv_s.dtype
+            )
+
+        @pl.when(e < n - 1)
+        def got_after():
+            halo_before.wait_recv()
+
+        both_orders(0, WINDOW)
+        both_orders(seq_rows + WINDOW, WINDOW)
+
     loads[1].wait()
-
-    @pl.when(e == 0)
-    def no_before():
-        kv_s[0:WINDOW, :] = jnp.zeros((WINDOW, kv_s.shape[1]), kv_s.dtype)
-
-    @pl.when(e > 0)
-    def got_before():
-        halo_after.wait_recv()
-
-    @pl.when(e == n - 1)
-    def no_after():
-        kv_s[seq_rows + WINDOW : seq_rows + 2 * WINDOW, :] = jnp.zeros(
-            (WINDOW, kv_s.shape[1]), kv_s.dtype
-        )
-
-    @pl.when(e < n - 1)
-    def got_after():
-        halo_before.wait_recv()
-
-    for kv_head in range(kv_heads):
-        lanes = slice(kv_head * 2 * HEAD_DIM, (kv_head + 1) * 2 * HEAD_DIM)
-        both = kv_s[:, lanes]
-        vk_s[:, lanes] = jnp.concatenate([both[:, HEAD_DIM:], both[:, :HEAD_DIM]], 1)
+    both_orders(WINDOW, seq_rows)
     loads[2].wait()
 
     span = STEP_ROWS + 2 * WINDOW
@@ -345,26 +353,32 @@
                     lower, results[0], results[1]
                 ).astype(jnp.bfloat16)
 
-    def attend_block(k):
-        owner = rem(t + k, tp)
-
+    def attend_inner(first, last):
         def step(i, carry):
-            attend_step(owner * own_count + i * STEP_ROWS)
+            attend_step(i * STEP_ROWS)
             return carry
 
-        lax.fori_loop(0, own_count // STEP_ROWS, step, 0)
-        block = att.at[at(owner * own_count, own_count), :]
-        if k == 0:
-            pltpu.make_async_copy(block, att_in.at[t], att_recv.at[0]).start()
-        else:
-            remote(block, att_in.at[t], att_send.at[k], att_recv.at[k], tp=owner).start()
-
-    def relay_tables():
-        for s in range(2):
-            arrived(info_in.at[s], info_recv.at[s])
-            table = info_in[s]
-            sel[s] = pick(table)
-            mixture(table, s)
+        lax.fori_loop(first, last, step, 0)
+
+    def attend_edges():
+        def step(i, carry):
+            attend_step(i * (seq_rows - STEP_ROWS))
+            return carry
+
+        lax.fori_loop(0, 2, step, 0)
+        for k in range(tp):
+            owner = rem(t + k, tp)
+            block = att.at[at(owner * own_count, own_count), :]
+            if k:
+                remote(block, att_in.at[t], att_send.at[k], att_recv.at[k], tp=owner).start()
+            else:
+                pltpu.make_async_copy(block, att_in.at[t], att_recv.at[0]).start()
+
+    def relay_tables(s):
+        arrived(info_in.at[s], info_recv.at[s])
+        table = info_in[s]
+        sel[s] = pick(table)
+        mixture(table, s)
 
     def relay_forward(s, c):
         arrived(block_in.at[s, c], block_recv.at[s, c])
@@ -383,6 +397,9 @@
 
     def on_relay(task, *args):
         pl.when(is_relay)(lambda: task(*args))
+
+    def off_relay(task, *args):
+        pl.when(jnp.logical_not(is_relay))(lambda: task(*args))
 
     def forward_weights(i):
         arrived(w_place(i, side), w_recv.at[i, side])
@@ -422,25 +439,26 @@
         res[c, at(first, group), :] = jnp.dot(
             hid[at(first, group), :], down_s[c], preferred_element_type=jnp.float32
         ).astype(jnp.bfloat16)
+        landing = relay_in.at[s, c, at(local * stride, stride), :]
         for k in range(members):
             block = res.at[c, at(far_source(s, k) * stride, stride), :]
-            landing = relay_in.at[s, c, at(local * stride, stride), :]
-            relay = own_relay_plane * members + rem(member + k, members)
             if k:
                 remote(
-                    block, landing, back_far_send.at[s, c], relay_recv.at[s, c], ep=relay
+                    block, landing, back_far_send.at[s, c], relay_recv.at[s, c],
+                    ep=plane * members + rem(member + k, members),
                 ).start()
             else:
-
-                @pl.when(is_relay)
-                def keep():
-                    pltpu.make_async_copy(block, landing, relay_recv.at[s, c]).start()
-
-                @pl.when(jnp.logical_not(is_relay))
-                def send():
-                    remote(
-                        block, landing, back_own_send.at[s, c], relay_recv.at[s, c], ep=relay
-                    ).start()
+                pltpu.make_async_copy(block, landing, relay_recv.at[s, c]).start()
+
+    def edge_block(s, c):
+        return relay_in.at[s, c, at(rem(plane, 2) * group, group), :]
+
+    def edge_forward(s, c):
+        arrived(edge_block(s, c), relay_recv.at[s, c])
+        remote(
+            edge_block(s, c), edge_block(s, c), edge_send.at[s, c], relay_recv.at[s, c],
+            ep=own_relay_plane * members + member,
+        ).start()
 
     def near_results(c):
         first = half * rows
@@ -480,25 +498,25 @@
             out_v.at[:, cols(c)], out_hbm.at[:, cols(c)], store_sem.at[c]
         ).start()
 
-    on_relay(relay_tables)
-    attend_block(1)
-    for c in range(0, 2):
-        on_relay(relay_forward, 0, c)
-    attend_block(2)
-    for c in range(2, 4):
-        on_relay(relay_forward, 0, c)
-    for k in range(3, tp):
-        attend_block(k)
-    on_relay(relay_forward, 0, 4)
-    attend_block(0)
-    for c in range(5, CHUNKS):
-        on_relay(relay_forward, 0, c)
+    on_relay(relay_tables, 0)
+    steps = seq_rows // STEP_ROWS
+    quarter = max(steps // 4, 1)
+    bounds = [1] + [min(1 + quarter * (i + 1), steps - 1) for i in range(4)]
+    plan = [range(0, 2), range(2, 4), range(4, 6), range(6, CHUNKS)]
+    for i in range(4):
+        attend_inner(bounds[i], bounds[i + 1])
+        for c in plan[i]:
+            on_relay(relay_forward, 0, c)
     forward_weights(0)
+    on_relay(relay_tables, 1)
+    on_relay(relay_forward, 1, 0)
+    got_halo()
+    attend_edges()
+    for c in range(1, 4):
+        on_relay(relay_forward, 1, c)
     for slot in range(side):
         for item in range(2):
             got_weights(item, slot)
-    for c in range(0, 4):
-        on_relay(relay_forward, 1, c)
     first_rows, last_rows = far_plane(0) * group, far_plane(1) * group
     arrived(x_in.at[at(first_rows, group), :], pack_recv.at[0])
     for slot in range(side):
@@ -513,6 +531,7 @@
     hidden_rows(first_rows, group, side)
     for c in range(7, CHUNKS):
         on_relay(relay_forward, 1, c)
+    hidden_rows(half * rows, rows, side)
     for slot in range(side + 1, tp):
         for item in range(2):
             got_weights(item, slot)
@@ -524,19 +543,25 @@
                 got_weights(2 + c, slot)
 
     forward_weights(2)
-    hidden_rows(half * rows, rows, side)
+    for slot in range(side + 1, tp):
+        hidden_rows(half * rows, rows, slot)
     got_down(0)
     results(0, 0)
+    on_relay(near_results, 0)
     forward_weights(3)
-    for slot in range(side + 1, tp):
-        hidden_rows(half * rows, rows, slot)
     got_down(1)
     results(0, 1)
+    on_relay(near_results, 1)
+    edges = [(0, 0), (0, 1), (1, 0), (1, 1)] + [
+        (s, c) for c in range(2, CHUNKS) for s in range(2)
+    ]
+    off_relay(edge_forward, *edges.pop(0))
     arrived(x_in.at[at(last_rows, group), :], pack_recv.at[1])
     for slot in range(tp):
         hidden_rows(last_rows, group, slot)
     results(1, 0)
     results(1, 1)
+    off_relay(edge_forward, *edges.pop(0))
     merges = [(0, 0), (0, 1), (1, 0), (1, 1)] + [
         (s, c) for c in range(2, CHUNKS) for s in range(2)
     ]
@@ -546,11 +571,16 @@
         got_down(c)
         results(0, c)
         results(1, c)
+        for _ in range(2):
+            off_relay(edge_forward, *edges.pop(0))
+        on_relay(near_results, c)
         for _ in range(due.get(c, 0)):
             on_relay(relay_merge, *merges.pop(0))
+    for item in edges:
+        off_relay(edge_forward, *item)
     for c in range(0, CHUNKS, 2):
-        near_results(c)
-        near_results(c + 1)
+        off_relay(near_results, c)
+        off_relay(near_results, c + 1)
         on_relay(relay_merge, *merges.pop(0))
     project()
     for item in merges:
@@ -598,7 +628,7 @@
         @pl.when(jnp.logical_not(is_relay))
         def sent_own():
             for s in range(2):
-                sent(res.at[c, pl.ds(0, stride), :], back_own_send.at[s, c])
+                sent(relay_in.at[s, c, pl.ds(0, group), :], edge_send.at[s, c])
 
 
 def body(

time: 129 us -> 123 us (0.953)
  the two profiles are of different devices: /device:TPU:0 before, /device:TPU:9 now
where the time goes in v2:
time: 123 us; the launch traced here: 122 us
  Pallas kernels  117 us (95%)
  local copies, waits for them, and re-layouts  4.22 us (3%)
    pallas_call x1, Pallas kernels, body(): pl.pallas_call(functools.partial(layer_kernel, n, tp, cap, stride), out_s...  117 us
    unnamed x4, local copies, waits for them, and re-layouts  4.22 us

profile of v2, /device:TPU:9, one launch (start us, length us, event | category | flops | bytes accessed | tf_op | source)
XLA Modules:
  0.0 122.4 jit_solution(12493883095771480307)
XLA Ops:
  0.6 117.5 %layer.1 = (bf16[512,2048]{1,0:T(8,128)(2,1)}, bf16[256,2048]{1,0:T(8,128)(2,1)}) custom-call(f32[16]{0:T(128)} %refs_0_.1, bf16[2048,256]{1,0:T(8,128)(2,1)} %refs_1_.1, bf16[2048,128]{1,0:T(8,128)(2,1)} %refs_2_.1, bf16[1024,2048]{1,0:T(8,128)(2,1)} %refs_3_.1, bf16[256,2048]{1,0:T(8,128)(2,1)} %refs_4_.1, f32[1,2048]{1,0:T(1,128)} %bitcast.9, ...), custom_call_target="tpu_custom_call" | custom-call | tf_op jit(solution)/shard_map/layer/pallas_call | solution.py:721
  118.1 0.0 copy-start
  118.1 3.2 %copy.15 = bf16[512,2048]{1,0:T(8,128)(2,1)} copy(bf16[512,2048]{1,0:T(8,128)(2,1)} %get-tuple-element.4) | data formatting | bytes 4194304
  121.4 0.0 copy-done
  121.4 1.0 copy.16
Async XLA Ops:
  118.1 3.3 %copy-start = (bf16[256,2048]{1,0:T(8,128)(2,1)S(1)}, bf16[256,2048]{1,0:T(8,128)(2,1)}, u32[]{:S(2)}) copy-start(bf16[256,2048]{1,0:T(8,128)(2,1)} %get-tuple-element.5) | copy-start | bytes 3145732

commit v3 on v2

--- a/solution.py
+++ b/solution.py
@@ -28,16 +28,16 @@
 def layer_kernel(n, tp, cap, stride, *refs):
     (
         sink, q_hbm, kv_hbm, ow_hbm, tok_hbm, gain, routes, rweights, gate_hbm, up_hbm, down_hbm,
-        mix_hbm, out_hbm,
+        mo_v, out_v,
         tok_v, norm_v, info, info_in, block_in, x_in, near_out, relay_out, sel,
         gate_s, up_s, down_s, hid, res, relay_in, merged, near_in, far_in,
-        mix_hi, mix_lo, out_v,
-        q_v, kv_s, vk_s, att, att_in, ow_v, mo_v,
+        mix_hi, mix_lo,
+        q_v, kv_s, vk_s, att, att_in, ow_v,
         load_sem, w_recv, w_near_send, w_far_send, w_fwd_send,
         halo_recv, halo_send, info_recv, info_send, block_recv, block_send,
         near_recv, near_send, pack_recv, pack_send,
         back_near_recv, back_near_send, back_far_send, edge_send,
-        relay_recv, merged_send, far_recv, att_recv, att_send, store_sem,
+        relay_recv, merged_send, far_recv, att_recv, att_send,
     ) = refs
     count, width = tok_v.shape
     wide = width // CHUNKS
@@ -432,7 +432,6 @@
                 for k in range(tp)
             )
             mo_v[:, cols(c)] = total.astype(jnp.bfloat16)
-        pltpu.make_async_copy(mo_v, mix_hbm, store_sem.at[CHUNKS]).start()
 
     def results(s, c):
         first = far_plane(s) * group
@@ -494,9 +493,6 @@
         total = mixed(2, near_in[c])
         arrived(far_in.at[c], far_recv.at[c])
         out_v[:, cols(c)] = (total + far_in[c].astype(jnp.float32)).astype(jnp.bfloat16)
-        pltpu.make_async_copy(
-            out_v.at[:, cols(c)], out_hbm.at[:, cols(c)], store_sem.at[c]
-        ).start()
 
     on_relay(relay_tables, 0)
     steps = seq_rows // STEP_ROWS
@@ -555,6 +551,7 @@
     edges = [(0, 0), (0, 1), (1, 0), (1, 1)] + [
         (s, c) for c in range(2, CHUNKS) for s in range(2)
     ]
+    off_relay(near_results, 0)
     off_relay(edge_forward, *edges.pop(0))
     arrived(x_in.at[at(last_rows, group), :], pack_recv.at[1])
     for slot in range(tp):
@@ -565,34 +562,27 @@
     merges = [(0, 0), (0, 1), (1, 0), (1, 1)] + [
         (s, c) for c in range(2, CHUNKS) for s in range(2)
     ]
-    due = {3: 3, 4: 1, 5: 1, 6: 2, 7: 1}
+    on_relay(relay_merge, *merges.pop(0))
     for c in range(2, CHUNKS):
         forward_weights(2 + c)
         got_down(c)
         results(0, c)
         results(1, c)
-        for _ in range(2):
+        for _ in range(1 + c % 2):
             off_relay(edge_forward, *edges.pop(0))
         on_relay(near_results, c)
-        for _ in range(due.get(c, 0)):
-            on_relay(relay_merge, *merges.pop(0))
+        on_relay(relay_merge, *merges.pop(0))
     for item in edges:
         off_relay(edge_forward, *item)
-    for c in range(0, CHUNKS, 2):
+    for c in range(1, CHUNKS):
         off_relay(near_results, c)
-        off_relay(near_results, c + 1)
+    while len(merges) > 4:
         on_relay(relay_merge, *merges.pop(0))
     project()
     for item in merges:
         on_relay(relay_merge, *item)
     for c in range(CHUNKS):
         finish(c)
-
-    for c in range(CHUNKS):
-        pltpu.make_async_copy(
-            out_v.at[:, cols(c)], out_hbm.at[:, cols(c)], store_sem.at[c]
-        ).wait()
-    pltpu.make_async_copy(mo_v, mix_hbm, store_sem.at[CHUNKS]).wait()
 
     def sent(ref, sem):
         pltpu.make_async_copy(ref, ref, sem).wait()
@@ -682,14 +672,12 @@
         vmem(CHUNKS, count, wide),
         vmem(3, count, rows),
         vmem(3, count, rows),
-        vmem(count, width),
         vmem(seq_rows, q_width),
         vmem(seq_rows + 2 * WINDOW, kv_width),
         vmem(seq_rows + 2 * WINDOW, kv_width),
         vmem(seq_rows, q_width),
         vmem(tp, seq_rows // tp, q_width),
         vmem(*out_weight.shape),
-        vmem(seq_rows // tp, width),
         dma((4,)),
         dma((items, tp)),
         dma((items, side)),
@@ -714,24 +702,23 @@
         dma((CHUNKS,)),
         dma((tp,)),
         dma((tp,)),
-        dma((CHUNKS + 1,)),
     ]
     anywhere = pl.BlockSpec(memory_space=pl.ANY)
     small = pl.BlockSpec(memory_space=pltpu.VMEM)
     return pl.pallas_call(
         functools.partial(layer_kernel, n, tp, cap, stride),
         out_shape=(
-            jax.ShapeDtypeStruct((seq_rows // tp, width), bf16),
-            jax.ShapeDtypeStruct((count, width), bf16),
+            pltpu.VMEM((seq_rows // tp, width), bf16),
+            pltpu.VMEM((count, width), bf16),
         ),
         in_specs=[
             pl.BlockSpec(memory_space=pltpu.SMEM), anywhere, anywhere, anywhere, anywhere,
             small, small, small, anywhere, anywhere, anywhere,
         ],
-        out_specs=(anywhere, anywhere),
+        out_specs=(small, small),
         scratch_shapes=scratch,
         compiler_params=pltpu.CompilerParams(
-            collective_id=0, has_side_effects=True, vmem_limit_bytes=67043328
+            collective_id=0, has_side_effects=True, vmem_limit_bytes=62000000
         ),
         name="layer",
     )(

time: 123 us -> 118 us (0.959)
  Pallas kernels: 117 us -> 115 us
  local copies, waits for them, and re-layouts: 4.22 us -> 2.29 us
    pallas_call x1, Pallas kernels: 117 us -> 115 us  [body(): pl.pallas_call(functools.partial(layer_kernel, n, tp, cap, stride), out_s...]
    unnamed x4 -> x2, local copies, waits for them, and re-layouts: 4.22 us -> 2.29 us
where the time goes in v3:
time: 118 us
  Pallas kernels  115 us (97%)
  local copies, waits for them, and re-layouts  2.29 us (2%)
    pallas_call x1, Pallas kernels, body(): pl.pallas_call(functools.partial(layer_kernel, n, tp, cap, stride), out_s...  115 us

profile of v3, /device:TPU:9, one launch (start us, length us, event | category | flops | bytes accessed | tf_op | source)
XLA Modules:
  0.0 118.1 jit_solution(6325729487553794208)
XLA Ops:
  0.6 115.1 %layer.1 = (bf16[512,2048]{1,0:T(8,128)(2,1)S(1)}, bf16[256,2048]{1,0:T(8,128)(2,1)S(1)}) custom-call(f32[16]{0:T(128)} %refs_0_.1, bf16[2048,256]{1,0:T(8,128)(2,1)} %refs_1_.1, bf16[2048,128]{1,0:T(8,128)(2,1)} %refs_2_.1, bf16[1024,2048]{1,0:T(8,128)(2,1)} %refs_3_.1, bf16[256,2048]{1,0:T(8,128)(2,1)} %refs_4_.1, f32[1,2048]{1,0:T(1,128)} %bitcast.9, ...), custom_call_target="tpu_custom_call" | custom-call | tf_op jit(solution)/shard_map/layer/pallas_call | solution.py:708
  115.8 1.3 %copy.15 = bf16[512,2048]{1,0:T(8,128)(2,1)} copy(bf16[512,2048]{1,0:T(8,128)(2,1)S(1)} %get-tuple-element.2) | data formatting | bytes 4194304
  117.1 1.0 copy.16

commit v4 on v3

--- a/solution.py
+++ b/solution.py
@@ -27,16 +27,17 @@
 
 def layer_kernel(n, tp, cap, stride, *refs):
     (
-        sink, q_hbm, kv_hbm, ow_hbm, tok_hbm, gain, routes, rweights, gate_hbm, up_hbm, down_hbm,
+        sink_hbm, q_hbm, kv_hbm, ow_hbm, tok_hbm, gain_hbm, routes_hbm, rweights_hbm,
+        gate_hbm, up_hbm, down_hbm,
         mo_v, out_v,
-        tok_v, norm_v, info, info_in, block_in, x_in, near_out, relay_out, sel,
+        sink, gain, routes, rweights, tok_v, norm_v, info, info_in, block_in, x_in, near_out, relay_out, sel,
         gate_s, up_s, down_s, hid, res, relay_in, merged, near_in, far_in,
         mix_hi, mix_lo,
         q_v, kv_s, vk_s, att, att_in, ow_v,
-        load_sem, w_recv, w_near_send, w_far_send, w_fwd_send,
+        load_sem, w_near_recv, w_recv, w_near_send, w_far_send, w_fwd_send,
         halo_recv, halo_send, info_recv, info_send, block_recv, block_send,
         near_recv, near_send, pack_recv, pack_send,
-        back_near_recv, back_near_send, back_far_send, edge_send,
+        back_near_recv, back_near_send, back_far_send, direct_send, edge_send,
         relay_recv, merged_send, far_recv, att_recv, att_send,
     ) = refs
     count, width = tok_v.shape
@@ -99,6 +100,10 @@
         pltpu.make_async_copy(kv_hbm, kv_own, load_sem.at[1]),
         pltpu.make_async_copy(q_hbm, q_v, load_sem.at[2]),
         pltpu.make_async_copy(ow_hbm, ow_v, load_sem.at[3]),
+        pltpu.make_async_copy(gain_hbm, gain, load_sem.at[4]),
+        pltpu.make_async_copy(routes_hbm, routes, load_sem.at[5]),
+        pltpu.make_async_copy(rweights_hbm, rweights, load_sem.at[6]),
+        pltpu.make_async_copy(sink_hbm, sink, load_sem.at[7]),
     ]
     items = 2 + CHUNKS
 
@@ -116,12 +121,14 @@
             return up_s.at[slot]
         return down_s.at[item - 2, pl.ds(slot * shard, shard), :]
 
+    def w_sem(item, slot):
+        if slot < side:
+            return w_near_recv.at[slot, 0 if item < 2 else 1]
+        return w_recv.at[item, slot - side]
+
     own_weights = [
-        pltpu.make_async_copy(w_source(i), w_place(i, 0), w_recv.at[i, 0]) for i in range(items)
+        pltpu.make_async_copy(w_source(i), w_place(i, 0), w_sem(i, 0)) for i in range(items)
     ]
-    for copy in loads:
-        copy.start()
-
     barrier = pltpu.get_barrier_semaphore()
 
     def greet(**where):
@@ -148,6 +155,9 @@
     @pl.when(jnp.logical_not(is_relay))
     def greet_relay():
         greet(ep=far_relay)
+
+    for copy in loads:
+        copy.start()
 
     def one(flag):
         return jnp.where(flag, 1, 0).astype(jnp.int32)
@@ -174,13 +184,13 @@
         halo_before.start()
 
     w_far = [
-        remote(w_source(i), w_place(i, side), w_far_send.at[i], w_recv.at[i, side], tp=tp_far)
+        remote(w_source(i), w_place(i, side), w_far_send, w_sem(i, side), tp=tp_far)
         for i in range(items)
     ]
     w_near = [
         remote(
-            w_source(i), w_place(i, (side - k) % side), w_near_send.at[i, k],
-            w_recv.at[i, (side - k) % side], tp=near_tp(k),
+            w_source(i), w_place(i, (side - k) % side), w_near_send.at[k],
+            w_sem(i, (side - k) % side), tp=near_tp(k),
         )
         for i in range(items)
         for k in range(1, side)
@@ -188,8 +198,8 @@
     w_fwd = {
         i: [
             remote(
-                w_place(i, side), w_place(i, side + (side - k) % side), w_fwd_send.at[i, k],
-                w_recv.at[i, side + (side - k) % side], tp=near_tp(k),
+                w_place(i, side), w_place(i, side + (side - k) % side), w_fwd_send.at[k],
+                w_sem(i, side + (side - k) % side), tp=near_tp(k),
             )
             for k in range(1, side)
         ]
@@ -199,6 +209,8 @@
         copy.start()
 
     loads[0].wait()
+    for copy in loads[4:]:
+        copy.wait()
     tokens = tok_v[...].astype(jnp.float32)
     centred = tokens - jnp.mean(tokens, -1, keepdims=True)
     scale = lax.rsqrt(jnp.mean(centred * centred, -1, keepdims=True) + 1e-06)
@@ -228,7 +240,7 @@
     send_info.start()
     send_blocks = [
         remote(
-            norm_v.at[c], block_in.at[slot_of, c], block_send.at[c], block_recv.at[slot_of, c],
+            norm_v.at[c], block_in.at[slot_of, c], block_send, block_recv.at[slot_of, c],
             ep=far_relay,
         )
         for c in range(CHUNKS)
@@ -370,9 +382,9 @@
             owner = rem(t + k, tp)
             block = att.at[at(owner * own_count, own_count), :]
             if k:
-                remote(block, att_in.at[t], att_send.at[k], att_recv.at[k], tp=owner).start()
+                remote(block, att_in.at[t], att_send, att_recv, tp=owner).start()
             else:
-                pltpu.make_async_copy(block, att_in.at[t], att_recv.at[0]).start()
+                pltpu.make_async_copy(block, att_in.at[t], att_recv).start()
 
     def relay_tables(s):
         arrived(info_in.at[s], info_recv.at[s])
@@ -389,7 +401,7 @@
         for j in range(1, half_count):
             remote(
                 relay_out.at[s, c, at(near_ep(j) * stride, stride), :], landing,
-                pack_send.at[s, c], pack_recv.at[s], ep=half * half_count + near_ep(j),
+                pack_send, pack_recv.at[s], ep=half * half_count + near_ep(j),
             ).start()
         pltpu.make_async_copy(
             relay_out.at[s, c, at(local * stride, stride), :], landing, pack_recv.at[s]
@@ -402,7 +414,7 @@
         pl.when(jnp.logical_not(is_relay))(lambda: task(*args))
 
     def forward_weights(i):
-        arrived(w_place(i, side), w_recv.at[i, side])
+        arrived(w_place(i, side), w_sem(i, side))
         for copy in w_fwd[i]:
             copy.start()
 
@@ -415,12 +427,10 @@
         ).astype(jnp.bfloat16)
 
     def got_weights(item, slot):
-        arrived(w_place(item, slot), w_recv.at[item, slot])
+        arrived(w_place(item, slot), w_sem(item, slot))
 
     def project():
-        arrived(att_in.at[0], att_recv.at[0])
-        for k in range(1, tp):
-            arrived(att_in.at[0], att_recv.at[k])
+        arrived(att_in, att_recv)
         loads[3].wait()
         total = jnp.zeros(mo_v.shape, jnp.float32)
         for c in range(CHUNKS):
@@ -433,7 +443,7 @@
             )
             mo_v[:, cols(c)] = total.astype(jnp.bfloat16)
 
-    def results(s, c):
+    def results(s, c, direct=False):
         first = far_plane(s) * group
         res[c, at(first, group), :] = jnp.dot(
             hid[at(first, group), :], down_s[c], preferred_element_type=jnp.float32
@@ -441,13 +451,23 @@
         landing = relay_in.at[s, c, at(local * stride, stride), :]
         for k in range(members):
             block = res.at[c, at(far_source(s, k) * stride, stride), :]
+            near_plane = own_relay_plane if direct else plane
             if k:
                 remote(
-                    block, landing, back_far_send.at[s, c], relay_recv.at[s, c],
-                    ep=plane * members + rem(member + k, members),
+                    block, landing, back_far_send, relay_recv.at[s, c],
+                    ep=near_plane * members + rem(member + k, members),
                 ).start()
             else:
-                pltpu.make_async_copy(block, landing, relay_recv.at[s, c]).start()
+                keep = pltpu.make_async_copy(block, landing, relay_recv.at[s, c])
+            if not k and direct:
+                hand = remote(
+                    block, landing, direct_send, relay_recv.at[s, c],
+                    ep=own_relay_plane * members + member,
+                )
+                pl.when(is_relay)(keep.start)
+                pl.when(jnp.logical_not(is_relay))(hand.start)
+            elif not k:
+                keep.start()
 
     def edge_block(s, c):
         return relay_in.at[s, c, at(rem(plane, 2) * group, group), :]
@@ -455,7 +475,7 @@
     def edge_forward(s, c):
         arrived(edge_block(s, c), relay_recv.at[s, c])
         remote(
-            edge_block(s, c), edge_block(s, c), edge_send.at[s, c], relay_recv.at[s, c],
+            edge_block(s, c), edge_block(s, c), edge_send, relay_recv.at[s, c],
             ep=own_relay_plane * members + member,
         ).start()
 
@@ -469,7 +489,7 @@
             target = half * half_count + near_ep(j)
             remote(
                 res.at[c, at(target * stride, stride), :], landing,
-                back_near_send.at[c], back_near_recv.at[c], ep=target,
+                back_near_send, back_near_recv.at[c], ep=target,
             ).start()
         pltpu.make_async_copy(
             res.at[c, own_rows, :], landing, back_near_recv.at[c]
@@ -484,7 +504,7 @@
         arrived(relay_in.at[s, c], relay_recv.at[s, c])
         merged[s, c] = mixed(s, relay_in[s, c]).astype(jnp.bfloat16)
         remote(
-            merged.at[s, c], far_in.at[c], merged_send.at[s, c], far_recv.at[c],
+            merged.at[s, c], far_in.at[c], merged_send, far_recv.at[c],
             ep=far_source(s, 0),
         ).start()
 
@@ -511,8 +531,7 @@
     for c in range(1, 4):
         on_relay(relay_forward, 1, c)
     for slot in range(side):
-        for item in range(2):
-            got_weights(item, slot)
+        arrived(gate_s.at[pl.ds(0, 2)], w_near_recv.at[slot, 0])
     first_rows, last_rows = far_plane(0) * group, far_plane(1) * group
     arrived(x_in.at[at(first_rows, group), :], pack_recv.at[0])
     for slot in range(side):
@@ -535,40 +554,38 @@
 
     def got_down(c):
         for slot in range(tp):
-            if slot != side:
+            if slot < side and c == 0:
+                arrived(gate_s.at[0], w_near_recv.at[slot, 1])
+            if slot > side:
                 got_weights(2 + c, slot)
 
+    directs = ((0, 0), (0, 1), (1, 0), (1, 1))
+    order = [(0, 0), (0, 1), (1, 0), (1, 1)] + [(s, c) for c in range(2, CHUNKS) for s in range(2)]
+    merges, edges = list(order), [item for item in order if item not in directs]
     forward_weights(2)
+    got_down(0)
+    results(0, 0, True)
+    forward_weights(3)
     for slot in range(side + 1, tp):
         hidden_rows(half * rows, rows, slot)
-    got_down(0)
-    results(0, 0)
-    on_relay(near_results, 0)
-    forward_weights(3)
     got_down(1)
-    results(0, 1)
-    on_relay(near_results, 1)
-    edges = [(0, 0), (0, 1), (1, 0), (1, 1)] + [
-        (s, c) for c in range(2, CHUNKS) for s in range(2)
-    ]
-    off_relay(near_results, 0)
-    off_relay(edge_forward, *edges.pop(0))
+    results(0, 1, True)
+    near_results(0)
     arrived(x_in.at[at(last_rows, group), :], pack_recv.at[1])
     for slot in range(tp):
         hidden_rows(last_rows, group, slot)
-    results(1, 0)
-    results(1, 1)
-    off_relay(edge_forward, *edges.pop(0))
-    merges = [(0, 0), (0, 1), (1, 0), (1, 1)] + [
-        (s, c) for c in range(2, CHUNKS) for s in range(2)
-    ]
+        if slot == side - 1:
+            on_relay(relay_merge, *merges.pop(0))
+    results(1, 0, True)
+    results(1, 1, True)
+    on_relay(near_results, 1)
     on_relay(relay_merge, *merges.pop(0))
     for c in range(2, CHUNKS):
         forward_weights(2 + c)
         got_down(c)
         results(0, c)
         results(1, c)
-        for _ in range(1 + c % 2):
+        for _ in range((0, 1, 2, 1, 2, 2)[min(c - 2, 5)]):
             off_relay(edge_forward, *edges.pop(0))
         on_relay(near_results, c)
         on_relay(relay_merge, *merges.pop(0))
@@ -595,30 +612,28 @@
     def sent_before():
         halo_before.wait_send()
 
-    for copy in w_far + w_near + [c for i in range(items) for c in w_fwd[i]]:
-        copy.wait_send()
+    whole_shard = gate_s.at[pl.ds(0, 3)]
+    sent(whole_shard, w_far_send)
+    for k in range(1, side):
+        sent(whole_shard, w_near_send.at[k])
+        sent(whole_shard, w_fwd_send.at[k])
     send_info.wait_send()
-    for copy in send_blocks:
-        copy.wait_send()
+    sent(norm_v, block_send)
     others = half_count - 1
     sent(near_out.at[pl.ds(0, others * stride), :], near_send)
-    for k in range(1, tp):
-        sent(att_in.at[0], att_send.at[k])
-    for c in range(CHUNKS):
-        sent(near_in.at[c, pl.ds(0, others * stride), :], back_near_send.at[c])
-        for s in range(2):
-            sent(res.at[c, pl.ds(0, (members - 1) * stride), :], back_far_send.at[s, c])
-
-        @pl.when(is_relay)
-        def sent_relay():
-            for s in range(2):
-                sent(relay_out.at[s, c, pl.ds(0, others * stride), :], pack_send.at[s, c])
-                sent(merged.at[s, c], merged_send.at[s, c])
-
-        @pl.when(jnp.logical_not(is_relay))
-        def sent_own():
-            for s in range(2):
-                sent(relay_in.at[s, c, pl.ds(0, group), :], edge_send.at[s, c])
+    sent(att_in.at[pl.ds(0, tp - 1)], att_send)
+    sent(near_in.at[:, pl.ds(0, others * stride), :], back_near_send)
+    sent(relay_in.at[:, :, pl.ds(0, (members - 1) * stride), :], back_far_send)
+
+    @pl.when(is_relay)
+    def sent_relay():
+        sent(relay_out.at[:, :, pl.ds(0, others * stride), :], pack_send)
+        sent(merged, merged_send)
+
+    @pl.when(jnp.logical_not(is_relay))
+    def sent_edge():
+        sent(relay_in.at[:, pl.ds(0, 2), pl.ds(0, stride), :], direct_send)
+        sent(relay_in.at[:, pl.ds(0, CHUNKS - 2), pl.ds(0, group), :], edge_send)
 
 
 def body(
@@ -652,6 +667,10 @@
         return pltpu.VMEM(shape, dtype)
 
     scratch = [
+        pltpu.SMEM(sink_logits.shape, f32),
+        vmem(1, width, dtype=f32),
+        vmem(TOPK, count, dtype=jnp.int32),
+        vmem(TOPK, count, dtype=f32),
         vmem(count, width),
         vmem(CHUNKS, count, wide),
         vmem(8, count, dtype=f32),
@@ -678,30 +697,32 @@
         vmem(seq_rows, q_width),
         vmem(tp, seq_rows // tp, q_width),
         vmem(*out_weight.shape),
-        dma((4,)),
-        dma((items, tp)),
+        dma((8,)),
+        dma((side, 2)),
         dma((items, side)),
-        dma((items,)),
-        dma((items, side)),
+        dma((side,)),
+        dma,
+        dma((side,)),
         dma((2,)),
         dma((2,)),
         dma((2,)),
         dma,
         dma((2, CHUNKS)),
+        dma,
+        dma,
+        dma,
+        dma((2,)),
+        dma,
         dma((CHUNKS,)),
         dma,
         dma,
-        dma((2,)),
+        dma,
+        dma,
         dma((2, CHUNKS)),
+        dma,
         dma((CHUNKS,)),
-        dma((CHUNKS,)),
-        dma((2, CHUNKS)),
-        dma((2, CHUNKS)),
-        dma((2, CHUNKS)),
-        dma((2, CHUNKS)),
-        dma((CHUNKS,)),
-        dma((tp,)),
-        dma((tp,)),
+        dma,
+        dma,
     ]
     anywhere = pl.BlockSpec(memory_space=pl.ANY)
     small = pl.BlockSpec(memory_space=pltpu.VMEM)
@@ -711,10 +732,7 @@
             pltpu.VMEM((seq_rows // tp, width), bf16),
             pltpu.VMEM((count, width), bf16),
         ),
-        in_specs=[
-            pl.BlockSpec(memory_space=pltpu.SMEM), anywhere, anywhere, anywhere, anywhere,
-            small, small, small, anywhere, anywhere, anywhere,
-        ],
+        in_specs=[anywhere] * 11,
         out_specs=(small, small),
         scratch_shapes=scratch,
         compiler_params=pltpu.CompilerParams(

time: 118 us -> 113 us (0.958)
  Pallas kernels: 115 us -> 110 us
    pallas_call x1, Pallas kernels: 115 us -> 110 us  [body(): pl.pallas_call(functools.partial(layer_kernel, n, tp, cap, stride), out_s...]
where the time goes in v4:
time: 113 us
  Pallas kernels  110 us (97%)
  local copies, waits for them, and re-layouts  2.29 us (2%)
    pallas_call x1, Pallas kernels, body(): pl.pallas_call(functools.partial(layer_kernel, n, tp, cap, stride), out_s...  110 us
    unnamed x2, local copies, waits for them, and re-layouts  2.29 us

profile of v4, /device:TPU:9, one launch (start us, length us, event | category | flops | bytes accessed | tf_op | source)
XLA Modules:
  0.0 113.2 jit_solution(1643934801949540265)
XLA Ops:
  0.6 110.3 %layer.1 = (bf16[512,2048]{1,0:T(8,128)(2,1)S(1)}, bf16[256,2048]{1,0:T(8,128)(2,1)S(1)}) custom-call(f32[16]{0:T(128)} %refs_0_.1, bf16[2048,256]{1,0:T(8,128)(2,1)} %refs_1_.1, bf16[2048,128]{1,0:T(8,128)(2,1)} %refs_2_.1, bf16[1024,2048]{1,0:T(8,128)(2,1)} %refs_3_.1, bf16[256,2048]{1,0:T(8,128)(2,1)} %refs_4_.1, f32[1,2048]{1,0:T(1,128)} %bitcast.9, ...), custom_call_target="tpu_custom_call" | custom-call | tf_op jit(solution)/shard_map/layer/pallas_call | solution.py:729
  110.9 1.3 %copy.15 = bf16[512,2048]{1,0:T(8,128)(2,1)} copy(bf16[512,2048]{1,0:T(8,128)(2,1)S(1)} %get-tuple-element.2) | data formatting | bytes 4194304
  112.2 1.0 copy.16

commit v5 on v4

--- a/solution.py
+++ b/solution.py
@@ -562,23 +562,35 @@
     directs = ((0, 0), (0, 1), (1, 0), (1, 1))
     order = [(0, 0), (0, 1), (1, 0), (1, 1)] + [(s, c) for c in range(2, CHUNKS) for s in range(2)]
     merges, edges = list(order), [item for item in order if item not in directs]
+    def last_arrived():
+        arrived(x_in.at[at(last_rows, group), :], pack_recv.at[1])
+
+    def last_hidden(*slots):
+        for slot in slots:
+            hidden_rows(last_rows, group, slot)
+
+    def near_hidden():
+        for slot in range(side + 1, tp):
+            hidden_rows(half * rows, rows, slot)
+
     forward_weights(2)
+    on_relay(last_arrived)
+    on_relay(last_hidden, *range(side))
     got_down(0)
     results(0, 0, True)
     forward_weights(3)
-    for slot in range(side + 1, tp):
-        hidden_rows(half * rows, rows, slot)
+    on_relay(last_hidden, *range(side, tp))
+    off_relay(near_hidden)
     got_down(1)
     results(0, 1, True)
-    near_results(0)
-    arrived(x_in.at[at(last_rows, group), :], pack_recv.at[1])
-    for slot in range(tp):
-        hidden_rows(last_rows, group, slot)
-        if slot == side - 1:
-            on_relay(relay_merge, *merges.pop(0))
+    off_relay(near_results, 0)
+    off_relay(last_arrived)
+    off_relay(last_hidden, *range(tp))
     results(1, 0, True)
     results(1, 1, True)
-    on_relay(near_results, 1)
+    on_relay(relay_merge, *merges.pop(0))
+    on_relay(near_hidden)
+    off_relay(near_results, 1)
     on_relay(relay_merge, *merges.pop(0))
     for c in range(2, CHUNKS):
         forward_weights(2 + c)
@@ -587,12 +599,15 @@
         results(1, c)
         for _ in range((0, 1, 2, 1, 2, 2)[min(c - 2, 5)]):
             off_relay(edge_forward, *edges.pop(0))
-        on_relay(near_results, c)
-        on_relay(relay_merge, *merges.pop(0))
+        for _ in range((1, 1, 2, 1, 2, 1)[min(c - 2, 5)]):
+            on_relay(relay_merge, *merges.pop(0))
+        on_relay(near_results, c - 2)
     for item in edges:
         off_relay(edge_forward, *item)
-    for c in range(1, CHUNKS):
+    for c in range(2, CHUNKS):
         off_relay(near_results, c)
+    for c in range(CHUNKS - 2, CHUNKS):
+        on_relay(near_results, c)
     while len(merges) > 4:
         on_relay(relay_merge, *merges.pop(0))
     project()

time: 113 us -> 113 us (level)
  no operation moved by 1% of the time
where the time goes in v5:
time: 113 us; the launch traced here: 112 us
  Pallas kernels  109 us (96%)
  local copies, waits for them, and re-layouts  2.29 us (2%)
    pallas_call x1, Pallas kernels, body(): pl.pallas_call(functools.partial(layer_kernel, n, tp, cap, stride), out_s...  109 us
    unnamed x2, local copies, waits for them, and re-layouts  2.29 us

profile of v5, /device:TPU:9, one launch (start us, length us, event | category | flops | bytes accessed | tf_op | source)
XLA Modules:
  0.0 112.2 jit_solution(17466566633357896233)
XLA Ops:
  0.6 109.3 %layer.1 = (bf16[512,2048]{1,0:T(8,128)(2,1)S(1)}, bf16[256,2048]{1,0:T(8,128)(2,1)S(1)}) custom-call(f32[16]{0:T(128)} %refs_0_.1, bf16[2048,256]{1,0:T(8,128)(2,1)} %refs_1_.1, bf16[2048,128]{1,0:T(8,128)(2,1)} %refs_2_.1, bf16[1024,2048]{1,0:T(8,128)(2,1)} %refs_3_.1, bf16[256,2048]{1,0:T(8,128)(2,1)} %refs_4_.1, f32[1,2048]{1,0:T(1,128)} %bitcast.9, ...), custom_call_target="tpu_custom_call" | custom-call | tf_op jit(solution)/shard_map/layer/pallas_call | solution.py:744
  109.9 1.3 %copy.15 = bf16[512,2048]{1,0:T(8,128)(2,1)} copy(bf16[512,2048]{1,0:T(8,128)(2,1)S(1)} %get-tuple-element.2) | data formatting | bytes 4194304
  111.2 1.0 copy.16

commit v6 on v5

--- a/solution.py
+++ b/solution.py
@@ -559,7 +559,7 @@
             if slot > side:
                 got_weights(2 + c, slot)
 
-    directs = ((0, 0), (0, 1), (1, 0), (1, 1))
+    directs = tuple((s, c) for c in range(3) for s in range(2))
     order = [(0, 0), (0, 1), (1, 0), (1, 1)] + [(s, c) for c in range(2, CHUNKS) for s in range(2)]
     merges, edges = list(order), [item for item in order if item not in directs]
     def last_arrived():
@@ -595,9 +595,9 @@
     for c in range(2, CHUNKS):
         forward_weights(2 + c)
         got_down(c)
-        results(0, c)
-        results(1, c)
-        for _ in range((0, 1, 2, 1, 2, 2)[min(c - 2, 5)]):
+        results(0, c, (0, c) in directs)
+        results(1, c, (1, c) in directs)
+        for _ in range((0, 0, 1, 2, 2, 2)[min(c - 2, 5)]):
             off_relay(edge_forward, *edges.pop(0))
         for _ in range((1, 1, 2, 1, 2, 1)[min(c - 2, 5)]):
             on_relay(relay_merge, *merges.pop(0))
@@ -647,8 +647,8 @@
 
     @pl.when(jnp.logical_not(is_relay))
     def sent_edge():
-        sent(relay_in.at[:, pl.ds(0, 2), pl.ds(0, stride), :], direct_send)
-        sent(relay_in.at[:, pl.ds(0, CHUNKS - 2), pl.ds(0, group), :], edge_send)
+        sent(relay_in.at[:, pl.ds(0, 3), pl.ds(0, stride), :], direct_send)
+        sent(relay_in.at[:, pl.ds(0, CHUNKS - 3), pl.ds(0, group), :], edge_send)
 
 
 def body(

time: 113 us -> 113 us (level)
  no operation moved by 1% of the time
where the time goes in v6:
time: 113 us; the launch traced here: 112 us
  Pallas kernels  109 us (96%)
  local copies, waits for them, and re-layouts  2.29 us (2%)
    pallas_call x1, Pallas kernels, body(): pl.pallas_call(functools.partial(layer_kernel, n, tp, cap, stride), out_s...  109 us
    unnamed x2, local copies, waits for them, and re-layouts  2.29 us

profile of v6, /device:TPU:9, one launch (start us, length us, event | category | flops | bytes accessed | tf_op | source)
XLA Modules:
  0.0 112.2 jit_solution(13929972848633174431)
XLA Ops:
  0.6 109.3 %layer.1 = (bf16[512,2048]{1,0:T(8,128)(2,1)S(1)}, bf16[256,2048]{1,0:T(8,128)(2,1)S(1)}) custom-call(f32[16]{0:T(128)} %refs_0_.1, bf16[2048,256]{1,0:T(8,128)(2,1)} %refs_1_.1, bf16[2048,128]{1,0:T(8,128)(2,1)} %refs_2_.1, bf16[1024,2048]{1,0:T(8,128)(2,1)} %refs_3_.1, bf16[256,2048]{1,0:T(8,128)(2,1)} %refs_4_.1, f32[1,2048]{1,0:T(1,128)} %bitcast.9, ...), custom_call_target="tpu_custom_call" | custom-call | tf_op jit(solution)/shard_map/layer/pallas_call | solution.py:744
  109.9 1.3 %copy.15 = bf16[512,2048]{1,0:T(8,128)(2,1)} copy(bf16[512,2048]{1,0:T(8,128)(2,1)S(1)} %get-tuple-element.2) | data formatting | bytes 4194304
  111.2 1.0 copy.16
